TPU v7x, 128 devices: a whole 4x4x4 slice. The times are simulated.
128 devices in a mesh: gr: 2 (over z_hi), sp: 32 (over z_lo, y, x), tp: 2 (over core).
Axes of the slice: x: 4, y: 4, z: 4 (z_hi: 2, z_lo: 2; z = z_hi * 2 + z_lo), core: 2. Of those that a mesh axis runs over, the one named last changes fastest.
Arguments:
- tokens: bfloat16 [2, 2, 24576, 2048], P('gr', 'tp', 'sp'), may hold values from -6 to 6
- key_weight: bfloat16 [2048, 2048], replicated, may hold values from -0.125 to 0.125
- value_weight: bfloat16 [2048, 2048], replicated, may hold values from -0.125 to 0.125
- cum_gate: float32 [2, 32, 2, 24576], P('gr', None, 'tp', 'sp'), may hold values from -49452 to 0, as said below
- query: bfloat16 [2, 32, 64], P('gr', 'sp'), may hold values from -12 to 12
Outputs:
- kv_cache: bfloat16 [2, 32, 49152, 128], P('gr', 'sp', 'tp')
- gate_cache: float32 [2, 32, 49152], P('gr', 'sp', 'tp')
- read: bfloat16 [2, 32, 64], P('gr', 'sp')
Inputs may be any that keep to these rules, and one draw needn't show every extreme that they name: `cum_gate`: each head's entries never rise along the positions.
All inputs are finite; a program needn't handle non-finite values.
Results may differ from a plain program's by a relative error of at most 0.012.
Values may be sent and summed in bfloat16 or wider, within the bound.
A program may use at most 128 MiB of HBM per device.

v0:
```python
import jax
import jax.numpy as jnp
from jax import lax
from jax.sharding import PartitionSpec as P


def cut_along(x, dim, length):
    before, after = (x.shape[:dim], x.shape[dim + 1 :])
    return jnp.moveaxis(x.reshape(*before, length, -1, *after), dim, 0)


def cut_rows(length, count):
    unit = 8 if length >= 8 * count else 1
    return [length // unit * k // count * unit for k in range(1, count)]


def joined_along(tiles, dim):
    tiles = jnp.moveaxis(tiles, 0, dim)
    dims = tiles.shape
    return tiles.reshape(*dims[:dim], dims[dim] * dims[dim + 1], *dims[dim + 2 :])


def exchange_in_pieces(x, axis, pieces, split_dim, concat_dim):
    tiles = cut_along(x, split_dim, lax.axis_size(axis))
    widest = max(range(1, max(2, tiles.ndim - 1)), key=lambda d: tiles.shape[d])
    outs = []
    for share in jnp.split(tiles, cut_rows(tiles.shape[widest], pieces), axis=widest):
        if share.size:
            outs.append(lax.all_to_all(share, axis, split_axis=0, concat_axis=0, tiled=True))
    return joined_along(jnp.concatenate(outs, axis=widest), concat_dim)


def gathered_once(x, axis):
    leaves = jax.tree.leaves(x)
    sequence = sorted(range(len(leaves)), key=lambda k: -leaves[k].size)
    width = (1, *leaves[sequence[0]].shape)[-1]
    lines = [
        jnp.pad(leaves[k].reshape(-1), (0, -leaves[k].size % width)).reshape(-1, width)
        for k in sequence
    ]
    both, at, found = (lax.all_gather(jnp.concatenate(lines), axis), 0, {})
    for k, line in zip(sequence, lines):
        share = both[:, at : at + len(line)].reshape(len(both), -1)
        found[k] = share[:, : leaves[k].size].reshape(-1, *leaves[k].shape)
        at += len(line)
    numbers = iter(range(len(leaves)))
    return jax.tree.map(lambda _: found[next(numbers)], x)


def combined_all(part, axis, combine):
    gathered = gathered_once(part, axis)

    def take(source):
        return jax.tree.map(lambda a: lax.dynamic_index_in_dim(a, source, 0, False), gathered)

    return lax.fori_loop(
        1, lax.axis_size(axis), lambda source, state: combine(state, take(source)), take(0)
    )


def combine_reads(first, second):
    top = jnp.maximum(first[0], second[0])
    scale_one = jnp.exp(first[0] - top)
    scale_two = jnp.exp(second[0] - top)
    total = first[1] * scale_one + second[1] * scale_two
    weighted = first[2] * scale_one[..., None] + second[2] * scale_two[..., None]
    return (top, total, weighted)


def partial_read(query, keys, values, gates, head_size):
    scores = jnp.einsum("bhe,bhse->bhs", query, keys, preferred_element_type=jnp.float32)
    scores = scores * head_size ** (-0.5) - gates
    top = jnp.max(scores, axis=-1)
    weights = jnp.exp(scores - top[..., None])
    total = jnp.sum(weights, axis=-1)
    weighted = jnp.einsum(
        "bhs,bhse->bhe", weights.astype(jnp.bfloat16), values, preferred_element_type=jnp.float32
    )
    return (top, total, weighted)


def local_project(tokens, key_weight, value_weight, head_size):
    width = tokens.shape[3]
    local_rows = tokens[:, 0]
    key_part = jnp.einsum(
        "btd,dhe->bhte",
        local_rows,
        key_weight.reshape(width, -1, head_size),
        preferred_element_type=jnp.float32,
    ).astype(jnp.bfloat16)
    value_part = jnp.einsum(
        "btd,dhe->bhte",
        local_rows,
        value_weight.reshape(width, -1, head_size),
        preferred_element_type=jnp.float32,
    ).astype(jnp.bfloat16)
    return (key_part, value_part)


def on_device(tokens, key_weight, value_weight, cum_gate, query):
    count = tokens.shape[0]
    head_size = query.shape[2]
    key_part = None
    value_part = None
    key_part, value_part = local_project(tokens, key_weight, value_weight, head_size)
    joined = jnp.concatenate([key_part, value_part], axis=-1)
    kv_cache = exchange_in_pieces(joined, "sp", 2, 1, 2)
    gates = lax.all_to_all(cum_gate, "sp", split_axis=1, concat_axis=3, tiled=True)
    gate_cache = gates.reshape(count, gates.shape[1], gates.shape[3])
    parts = partial_read(
        query, kv_cache[..., :head_size], kv_cache[..., head_size:], gate_cache, head_size
    )
    top, total, weighted = combined_all(parts, "tp", combine_reads)
    read = (weighted / total[..., None]).astype(jnp.bfloat16)
    return (kv_cache, gate_cache, read)


def solution(mesh):
    placed = (P("gr", "tp", "sp", None), P(), P(), P("gr", None, "tp", "sp"), P("gr", "sp", None))
    return jax.shard_map(
        on_device,
        mesh=mesh,
        in_specs=placed,
        out_specs=(P("gr", "sp", "tp", None), P("gr", "sp", "tp"), P("gr", "sp", None)),
        check_vma=False,
    )
```

profile of v0, /device:TPU:1, one launch (start us, length us, event | category | flops | bytes accessed | tf_op | source)
XLA Modules:
  0.0 169.5 jit_solution(5950905073197801298)
XLA Ops:
  0.6 0.0 copy-start
  0.6 9.5 %all-to-all-start.2 = ((f32[1,32,1,768]{3,2,0,1:T(1,128)}), f32[1,32,1,768]{3,2,0,1:T(1,128)S(1)}, u32[]{:S(2)}, u32[]{:S(2)}) async-start(f32[1,32,1,768]{3,2,0,1:T(1,128)} %bitcast.70), calls=%async_computation.2 | async-start | bytes 196608 | tf_op jit(solution)/shard_map/all_to_all | solution.py:108
  10.1 12.3 %copy.14 = bf16[2048,2048]{0,1:T(8,128)(2,1)} copy(bf16[2048,2048]{1,0:T(8,128)(2,1)} %param.7) | data formatting | bytes 16777216 | tf_op args[2]
  22.4 12.4 %copy.13 = bf16[2048,2048]{0,1:T(8,128)(2,1)} copy(bf16[2048,2048]{1,0:T(8,128)(2,1)} %param.6) | data formatting | bytes 16777216 | tf_op args[1]
  34.8 0.0 copy-done
  34.8 0.0 copy-start.3
  34.8 9.3 %convert_bitcast_fusion = bf16[1,32,768,64]{2,3,1,0:T(8,128)(2,1)S(1)} fusion(bf16[2048,32,64]{0,2,1:T(8,128)(2,1)} %bitcast.64, bf16[1,1,768,2048]{3,2,1,0:T(8,128)(2,1)S(1)} %copy-done), kind=kOutput, calls=%fused_computation.12 | convolution fusion | flops 6444023808 | bytes 14680064 | tf_op jit(solution)/shard_map/btd,dhe->bhte/dot_general | solution.py:91
  44.1 0.0 copy-done.3
  44.1 8.1 %convert_bitcast_fusion.1 = bf16[1,32,768,64]{2,3,1,0:T(8,128)(2,1)} fusion(bf16[2048,32,64]{0,2,1:T(8,128)(2,1)S(1)} %bitcast.63, bf16[1,1,768,2048]{3,2,1,0:T(8,128)(2,1)S(1)} %copy-done), kind=kOutput, calls=%fused_computation.13 | convolution fusion | flops 6444023808 | bytes 14680064 | tf_op jit(solution)/shard_map/btd,dhe->bhte/dot_general | solution.py:85
  52.1 2.5 %maximum_bitcast_fusion = bf16[32,1,1,768,128]{3,4,0,2,1:T(8,128)(2,1)S(1)} fusion(bf16[1,32,768,64]{2,3,1,0:T(8,128)(2,1)S(1)} %convert_bitcast_fusion, bf16[1,32,768,64]{2,3,1,0:T(8,128)(2,1)} %convert_bitcast_fusion.1), kind=kLoop, calls=%fused_computation.4 | loop fusion | flops 12582912 | bytes 12582912 | tf_op jit(solution)/shard_map/transpose;reshape | solution.py:9
  54.7 2.9 %slice_bitcast_fusion.5 = (bf16[32,1,1,384,128]{3,4,2,1,0:T(8,128)(2,1)S(1)}, bf16[32,1,1,384,128]{3,4,2,1,0:T(8,128)(2,1)}) fusion(bf16[32,1,1,768,128]{3,4,0,2,1:T(8,128)(2,1)S(1)} %maximum_bitcast_fusion), kind=kLoop, calls=%fused_computation.7 | loop fusion | bytes 12582912 | tf_op jit(solution)/shard_map/split | solution.py:27
  57.6 0.0 all-to-all-done.2
  57.6 44.9 %all_to_all.19 = bf16[32,1,1,384,128]{3,4,2,1,0:T(8,128)(2,1)} all-to-all(bf16[32,1,1,384,128]{3,4,2,1,0:T(8,128)(2,1)S(1)} %get-tuple-element.19), channel_id=1, replica_groups=mesh['gr'=2,'sp'=32,'tp'=2] {'sp'}, dimensions={0} | all-to-all | bytes 6291456 | tf_op jit(solution)/shard_map/all_to_all | solution.py:29
  102.5 4.9 %all-to-all-start.1 = ((bf16[32,1,1,384,128]{3,4,2,1,0:T(8,128)(2,1)}), bf16[32,1,1,384,128]{3,4,2,1,0:T(8,128)(2,1)S(1)}, u32[]{:S(2)}, u32[]{:S(2)}) async-start(bf16[32,1,1,384,128]{3,4,2,1,0:T(8,128)(2,1)} %get-tuple-element.20), calls=%async_computation.1 | async-start | bytes 6291456 | tf_op jit(solution)/shard_map/all_to_all | solution.py:29
  107.4 4.6 %copy.17 = bf16[32,1,1,384,128]{4,3,0,2,1:T(8,128)(2,1)} copy(bf16[32,1,1,384,128]{3,4,2,1,0:T(8,128)(2,1)} %all_to_all.19) | data formatting | bytes 6291456 | tf_op jit(solution)/shard_map/all_to_all | solution.py:29
  112.1 32.2 %all-to-all-done.1 = bf16[32,1,1,384,128]{3,4,2,1,0:T(8,128)(2,1)S(1)} async-done(((bf16[32,1,1,384,128]{3,4,2,1,0:T(8,128)(2,1)}), bf16[32,1,1,384,128]{3,4,2,1,0:T(8,128)(2,1)S(1)}, u32[]{:S(2)}, u32[]{:S(2)}) %all-to-all-start.1) | async-done | bytes 3145760 | tf_op jit(solution)/shard_map/all_to_all | solution.py:29
  144.2 2.8 %copy.18 = bf16[32,1,1,384,128]{4,3,0,2,1:T(8,128)(2,1)} copy(bf16[32,1,1,384,128]{3,4,2,1,0:T(8,128)(2,1)S(1)} %all-to-all-done.1) | data formatting | bytes 6291456 | tf_op jit(solution)/shard_map/all_to_all | solution.py:29
  147.1 0.0 copy-start.4
  147.1 3.5 %pad_maximum_fusion = bf16[32,1,1,768,128]{4,3,0,2,1:T(8,128)(2,1)S(1)} fusion(bf16[32,1,1,384,128]{4,3,0,2,1:T(8,128)(2,1)} %copy.18, bf16[32,1,1,384,128]{4,3,0,2,1:T(8,128)(2,1)} %copy.17), kind=kLoop, calls=%fused_computation.5 | loop fusion | flops 12582912 | bytes 12582912 | tf_op jit(solution)/shard_map/concatenate | solution.py:30
  150.6 0.0 copy-start.2
  150.6 0.0 copy-start.1
  150.6 0.0 copy-done.4
  150.6 1.7 %fusion.1 = f32[1,24576]{1,0:T(1,128)S(1)} fusion(bf16[1,1,24576,128]{3,2,1,0:T(8,128)(2,1)S(1)} %bitcast.60, bf16[1,1,64]{2,1,0:T(2,128)(2,1)S(1)} %copy-done.4), kind=kOutput, calls=%fused_computation.3 | convolution fusion | flops 3145728 | bytes 6389888 | tf_op jit(solution)/shard_map/bhe,bhse->bhs/dot_general | solution.py:71
  152.4 0.7 fusion.14
  153.0 2.1 %fusion.11 = (bf16[24576]{0:T(1024)(128)(2,1)S(1)}, f32[]{:T(128)}) fusion(f32[]{:T(128)} %fusion.14, f32[24576]{0:T(1024)S(1)} %bitcast.66, f32[24576]{0:T(1024)S(1)} %bitcast.69), kind=kLoop, calls=%fused_computation.17 | loop fusion | flops 122879 | bytes 245768 | tf_op jit(solution)/shard_map/convert_element_type | solution.py:77
  155.1 0.1 reshape.134
  155.2 1.8 %fusion = f32[1,64]{1,0:T(1,128)S(1)} fusion(bf16[24576,1]{0,1:T(2,128)(2,1)S(1)} %reshape.134, bf16[1,1,24576,128]{3,2,1,0:T(8,128)(2,1)S(1)} %bitcast.61), kind=kOutput, calls=%fused_computation.1 | convolution fusion | flops 3145728 | bytes 6340864 | tf_op jit(solution)/shard_map/bhs,bhse->bhe/dot_general | solution.py:76
  157.0 0.0 copy-done.2
  157.0 1.3 pad_bitcast_fusion
  158.4 4.9 %all-gather.1 = f32[2,3,64]{2,1,0:T(4,128)S(1)} all-gather(f32[1,3,64]{2,1,0:T(4,128)S(1)} %maximum_bitcast_fusion.1), channel_id=2, replica_groups=mesh['gr'=2,'sp'=32,'tp'=2] {'tp'}, dimensions={0}, use_global_device_ids=true | all-gather | bytes 2304 | tf_op jit(solution)/shard_map/all_gather | solution.py:41
  163.3 0.5 fusion.17
  166.4 0.5 fusion.16
  168.3 0.5 divide_convert_fusion
  168.8 0.6 copy.21
  169.5 0.0 copy-done.1
  (2 shorter events, 0.0 us)
Async XLA Ops:
  0.6 34.2 %copy-start = (bf16[1,1,768,2048]{3,2,1,0:T(8,128)(2,1)S(1)}, bf16[1,1,768,2048]{3,2,1,0:T(8,128)(2,1)}, u32[]{:S(2)}) copy-start(bf16[1,1,768,2048]{3,2,1,0:T(8,128)(2,1)} %param.5) | copy-start | bytes 9437188
  0.6 56.9 %all-to-all-start.2 = ((f32[1,32,1,768]{3,2,0,1:T(1,128)}), f32[1,32,1,768]{3,2,0,1:T(1,128)S(1)}, u32[]{:S(2)}, u32[]{:S(2)}) async-start(f32[1,32,1,768]{3,2,0,1:T(1,128)} %bitcast.70), calls=%async_computation.2 | async-start | bytes 196608 | tf_op jit(solution)/shard_map/all_to_all | solution.py:108
  34.8 9.3 %copy-start.3 = (bf16[2048,2048]{0,1:T(8,128)(2,1)S(1)}, bf16[2048,2048]{0,1:T(8,128)(2,1)}, u32[]{:S(2)}) copy-start(bf16[2048,2048]{0,1:T(8,128)(2,1)} %copy.13) | copy-start | bytes 25165828
  102.5 41.8 %all-to-all-start.1 = ((bf16[32,1,1,384,128]{3,4,2,1,0:T(8,128)(2,1)}), bf16[32,1,1,384,128]{3,4,2,1,0:T(8,128)(2,1)S(1)}, u32[]{:S(2)}, u32[]{:S(2)}) async-start(bf16[32,1,1,384,128]{3,4,2,1,0:T(8,128)(2,1)} %get-tuple-element.20), calls=%async_computation.1 | async-start | bytes 6291456 | tf_op jit(solution)/shard_map/all_to_all | solution.py:29
  147.1 3.6 %copy-start.4 = (bf16[1,1,64]{2,1,0:T(2,128)(2,1)S(1)}, bf16[1,1,64]{2,1,0:T(2,128)(2,1)}, u32[]{:S(2)}) copy-start(bf16[1,1,64]{2,1,0:T(2,128)(2,1)} %param.9) | copy-start | bytes 388
  150.6 6.4 %copy-start.2 = (bf16[32,1,1,768,128]{4,3,0,2,1:T(8,128)(2,1)}, bf16[32,1,1,768,128]{4,3,0,2,1:T(8,128)(2,1)S(1)}, u32[]{:S(2)}) copy-start(bf16[32,1,1,768,128]{4,3,0,2,1:T(8,128)(2,1)S(1)} %pad_maximum_fusion) | copy-start | bytes 18874372
  150.6 18.8 %copy-start.1 = (bf16[1,1,768,2048]{3,2,1,0:T(8,128)(2,1)S(1)}, bf16[1,1,768,2048]{3,2,1,0:T(8,128)(2,1)}, u32[]{:S(2)}) copy-start(bf16[1,1,768,2048]{3,2,1,0:T(8,128)(2,1)} %param.5) | copy-start | bytes 9437188
where the time goes:
time: 171 us; the launch traced here: 169 us
  blocking collectives  49.8 us (29%)
  local copies, waits for them, and re-layouts  38.1 us (22%)
  waiting for transfers between devices  32.2 us (19%)
  matrix products  20.9 us (12%)
  starting transfers between devices  14.4 us (8%)
  other arithmetic  9.36 us (5%)
  between operations  4.72 us (3%)
    all_to_all x1, blocking collectives, exchange_in_pieces(): lax.all_to_all(share, axis, split_axis=0, concat_axis=0, tiled=True)  44.9 us
    all_to_all x1, waiting for transfers between devices, exchange_in_pieces(): lax.all_to_all(share, axis, split_axis=0, concat_axis=0, tiled=True)  32.2 us
    unnamed x13, local copies, waits for them, and re-layouts  25.3 us
    all_to_all x1, starting transfers between devices, on_device(): lax.all_to_all(cum_gate, 'sp', split_axis=1, concat_axis=3, tiled=True)  9.49 us
    dot_general x1, matrix products, local_project(): jnp.einsum('btd,dhe->bhte', local_rows, value_weight.reshape(width, -1, h...  9.28 us
    dot_general x1, matrix products, local_project(): jnp.einsum('btd,dhe->bhte', local_rows, key_weight.reshape(width, -1, hea...  8.06 us
    all_to_all x2, local copies, waits for them, and re-layouts, exchange_in_pieces(): lax.all_to_all(share, axis, split_axis=0, concat_axis=0, tiled=True)  7.49 us
    all_to_all x1, starting transfers between devices, exchange_in_pieces(): lax.all_to_all(share, axis, split_axis=0, concat_axis=0, tiled=True)  4.92 us
  transfers between devices with their start and end apart: 2, of which 1 were waited for; matrix products, arithmetic and copies ran while one was open for 31% of the time, Pallas kernels for 0%

commit v1 on v0

v1 whole, which is shorter than its diff:
```python
import functools

import jax
import jax.numpy as jnp
from jax import lax
from jax.experimental import pallas as pl
from jax.experimental.pallas import tpu as pltpu
from jax.sharding import PartitionSpec as P

MESH = pl.DeviceIdType.MESH
NX, NY, NZ = 4, 4, 2
COLORS = 3
GROUPS = NY * NZ
NEAR = (1, 3, 2)
F32 = jnp.float32
BF16 = jnp.bfloat16


def group_step(g):
    h, r = g // 4, g % 4
    dy = (1 - h) * (1 + 2 * (r % 2)) + h * (2 - 2 * (r // 2))
    dz = (1 - h) * (1 - r // 2) + h * (1 - r % 2)
    return dy, dz


G_OF = {group_step(g): g for g in range(GROUPS)}


def exchange_kernel(
    tok_hbm, kw_hbm, vw_hbm, gate_hbm, q_ref,
    kv_ref, gate_ref, read_ref,
    tok, w, sr0, sr1, sr2, t0, t1, t2, gin, gr, gt, q8, m_ref, l_ref, a_ref, stat, peer,
    tok_sem, w_sem, gl_sem,
    s10, r10, s11, r11, s12, r12,
    s20, r20, s21, r21, s22, r22,
    s30, r30, s31, r31, s32, r32,
    sg1, rg1, sg2, rg2, sg3, rg3, st, rt,
):
    grp, sp, tp = (lax.axis_index(n) for n in ("gr", "sp", "tp"))
    x, y, z = sp % NX, (sp // NX) % NY, sp // (NX * NY)
    oz = 1 - z
    rows = tok.shape[0]
    unit = rows // COLORS
    half = q_ref.shape[-1]
    cols = w.shape[-1]
    scale = half ** (-0.5)

    def dev(xx, yy, zz):
        return (grp, zz * (NX * NY) + yy * NX + xx, tp)

    def px(d):
        return (x + d) % NX

    def py(d):
        return (y + d) % NY

    def send(src, dst, ssem, rsem, to):
        pltpu.make_async_remote_copy(
            src_ref=src, dst_ref=dst, send_sem=ssem, recv_sem=rsem, device_id=to, device_id_type=MESH
        ).start()

    def done(ref, sem):
        pltpu.make_async_copy(ref, ref, sem).wait()

    def weight_loads(g):
        dy, dz = group_step(g)
        at = (((z + dz) % NZ) * NY + py(dy)) * cols
        at = pl.multiple_of(at, cols)
        return (
            pltpu.make_async_copy(kw_hbm.at[:, pl.ds(at, cols)], w.at[g, 0], w_sem.at[g, 0]),
            pltpu.make_async_copy(vw_hbm.at[:, pl.ds(at, cols)], w.at[g, 1], w_sem.at[g, 1]),
        )

    tok_load = pltpu.make_async_copy(tok_hbm, tok, tok_sem)
    tok_load.start()
    for load in weight_loads(0):
        load.start()
    gate_loads = (
        pltpu.make_async_copy(gate_hbm, gin, gl_sem.at[0]),
        pltpu.make_async_copy(gate_hbm.at[:, :, x], gr.at[x], gl_sem.at[1]),
    )
    for load in gate_loads:
        load.start()
    for load in weight_loads(1):
        load.start()

    barrier = pltpu.get_barrier_semaphore()
    peers = [dev(px(d), y, z) for d in NEAR] + [dev(x, py(d), z) for d in NEAR]
    peers += [dev(x, y, oz), (grp, sp, 1 - tp)]
    for p in peers:
        pl.semaphore_signal(barrier, inc=1, device_id=p, device_id_type=MESH)

    query = jnp.concatenate([q_ref[...].astype(F32), jnp.zeros((1, half), F32)], axis=-1)
    q8[...] = jnp.broadcast_to(query, q8.shape).astype(BF16)
    m_ref[...] = jnp.full(m_ref.shape, -1e30, F32)
    l_ref[...] = jnp.zeros(l_ref.shape, F32)
    a_ref[...] = jnp.zeros(a_ref.shape, F32)

    lane = lax.broadcasted_iota(jnp.int32, (unit, 2 * half), 1)

    def compute(g):
        dy, dz = group_step(g)
        yb, zb = py(dy), (z + dz) % NZ
        slot1 = yb + NY * (1 - (dy + 3) // 4)
        slot2 = zb + NZ * (1 - dz)
        for load in weight_loads(g):
            load.wait()
        for c in range(COLORS):
            left = tok[c * unit : (c + 1) * unit, :]
            k = jnp.dot(left, w[g, 0], preferred_element_type=F32)
            v = jnp.dot(left, w[g, 1], preferred_element_type=F32)
            for j in range(NX):
                at = (j // 2) * 2 * half
                kk, vv = k[:, at : at + 2 * half], v[:, at : at + 2 * half]
                if j % 2 == 0:
                    both = jnp.where(lane < half, kk, pltpu.roll(vv, half, 1))
                else:
                    both = jnp.where(lane < half, pltpu.roll(kk, half, 1), vv)
                both = both.astype(BF16)
                if c == 0:
                    slot0 = j + NX * (1 - ((j + NX - x) % NX + NX - 1) // NX)
                    sr0[slot0, yb, zb] = both
                elif c == 1:
                    sr1[slot1, zb, j] = both
                else:
                    sr2[slot2, j, yb] = both

    def first_sends(g):
        dy, dz = group_step(g)
        yb, zb = py(dy), (z + dz) % NZ

        def along_y():
            send(sr1.at[yb, zb], sr1.at[NY + y, zb], s11.at[g], r11.at[g], dev(x, yb, z))

        def along_z():
            send(sr2.at[zb, :, yb], sr2.at[NZ + z, :, yb], s12.at[g], r12.at[g], dev(x, y, oz))

        if isinstance(g, int):
            if dy != 0:
                along_y()
            if dz != 0:
                along_z()
        else:
            pl.when(dy != 0)(along_y)
            pl.when(dz != 0)(along_z)
        for d in NEAR:
            send(sr0.at[px(d), yb, zb], sr0.at[NX + x, yb, zb], s10.at[g, d], r10.at[g, d], dev(px(d), y, z))

    tok_load.wait()
    compute(0)
    for load in weight_loads(2):
        load.start()
    pl.semaphore_wait(barrier, len(peers))
    first_sends(0)
    for load in gate_loads:
        load.wait()
    for d in NEAR:
        send(gin.at[:, :, px(d)], gr.at[x], sg1.at[d], rg1.at[d], dev(px(d), y, z))

    def step(g, carry):
        @pl.when(g < GROUPS - 2)
        def _():
            for load in weight_loads(g + 2):
                load.start()

        compute(g)
        first_sends(g)
        return carry

    lax.fori_loop(1, GROUPS, step, 0)

    def fwd0(dy, dx):
        sx = (x + NX - dx) % NX
        send(sr0.at[NX + sx, py(dy)], t0.at[y, sx], s20.at[dy, dx], r20.at[dy, dx], dev(x, py(dy), z))

    def fwd1(dy):
        sy = (y + NY - dy) % NY
        send(sr1.at[NY + sy, oz], t1.at[z, sy], s21.at[dy], r21.at[dy], dev(x, y, oz))

    def fwd2(dx, dz):
        sz = (z + dz) % NZ
        send(sr2.at[NZ + sz, px(dx)], t2.at[x, sz], s22.at[dx, dz], r22.at[dx, dz], dev(px(dx), y, z))

    def got10(dy, dz, dx):
        g = G_OF[(dy, dz)]
        done(sr0.at[NX + (x + NX - dx) % NX, py(dy), (z + dz) % NZ], r10.at[g, dx])

    def got11(dy, dz):
        g = G_OF[(dy, dz)]
        done(sr1.at[NY + (y + NY - dy) % NY, (z + dz) % NZ], r11.at[g])

    def got12(dy):
        g = G_OF[(dy, 1)]
        done(sr2.at[NZ + oz, :, py(dy)], r12.at[g])

    fwd1(0)
    for d in NEAR:
        fwd0(d, 0)
        fwd2(d, 0)
    for d in NEAR:
        done(gr.at[(x + NX - d) % NX], rg1.at[d])
    gt[y] = gr[:, :, y]
    got11(1, 1)
    fwd1(1)
    got11(3, 1)
    fwd1(3)
    for dx in NEAR:
        for dy in NEAR[:2]:
            got10(dy, 1, dx)
            got10(dy, 0, dx)
            fwd0(dy, dx)
    for d in NEAR:
        send(gr.at[:, :, py(d)], gt.at[y], sg2.at[d], rg2.at[d], dev(x, py(d), z))
    got11(2, 1)
    fwd1(2)
    for dx in NEAR:
        got10(2, 1, dx)
        got10(2, 0, dx)
        fwd0(2, dx)
    for dy in (1, 3, 2, 0):
        got12(dy)
    for dx in NEAR:
        fwd2(dx, 1)

    def out0(dy):
        sy = (y + NY - dy) % NY
        src = sr0.at[pl.ds(NX, NX), y, oz] if dy == 0 else t0.at[sy, :, oz]
        send(src, kv_ref.at[z, sy, :, 0], s30.at[dy], r30.at[dy], dev(x, y, oz))

    def out1(dz, dx):
        sz = (z + dz) % NZ
        src = sr1.at[pl.ds(NY, NY), z, px(dx)] if dz == 0 else t1.at[sz, :, px(dx)]
        send(src, kv_ref.at[sz, :, x, 1], s31.at[dz, dx], r31.at[dz, dx], dev(px(dx), y, z))

    def out2(dx, dy):
        sx = (x + NX - dx) % NX
        src = sr2.at[pl.ds(NZ, NZ), x, py(dy)] if dx == 0 else t2.at[sx, :, py(dy)]
        send(src, kv_ref.at[:, y, sx, 2], s32.at[dx, dy], r32.at[dx, dy], dev(x, py(dy), z))

    for dx in NEAR:
        got10(0, 1, dx)
    out0(0)
    for dy in NEAR:
        got11(dy, 0)
    for d in NEAR:
        out1(0, d)
        out2(0, d)
    for dx in NEAR:
        got10(0, 0, dx)

    def attend(kv, gate):
        s = lax.dot_general(q8[...], kv, (((1,), (1,)), ((), ())), preferred_element_type=F32)
        s = s * scale - gate
        old = m_ref[...]
        top = jnp.maximum(old, jnp.max(s, axis=1, keepdims=True))
        p = jnp.exp(s - top[:, :1])
        keep = jnp.exp(old - top)
        m_ref[...] = top
        l_ref[...] = l_ref[...] * keep + jnp.sum(p, axis=1, keepdims=True)
        a_ref[...] = a_ref[...] * keep + jnp.dot(p.astype(BF16), kv, preferred_element_type=F32)

    def attend0(sz, sy):
        kv = kv_ref[sz, sy, :, 0].reshape(NX * unit, 2 * half)
        gate = jnp.concatenate([gate_ref[sz, sy, k, :, 0:unit] for k in range(NX)], axis=-1)
        attend(kv, gate)

    def attend1(sz, sx):
        kv = kv_ref[sz, :, sx, 1].reshape(NY * unit, 2 * half)
        gate = jnp.concatenate([gate_ref[sz, k, sx, :, unit : 2 * unit] for k in range(NY)], axis=-1)
        attend(kv, gate)

    def attend2(sy, sx):
        kv = kv_ref[:, sy, sx, 2].reshape(NZ * unit, 2 * half)
        gate = jnp.concatenate([gate_ref[k, sy, sx, :, 2 * unit : 3 * unit] for k in range(NZ)], axis=-1)
        attend(kv, gate)

    def keep0(dy):
        sy = (y + NY - dy) % NY
        kv_ref[z, sy, :, 0] = sr0[NX : 2 * NX, y, z] if dy == 0 else t0[sy, :, z]

    def keep1(dz):
        sz = (z + dz) % NZ
        kv_ref[sz, :, x, 1] = sr1[NY : 2 * NY, z, x] if dz == 0 else t1[sz, :, x]

    def keep2(dx):
        sx = (x + NX - dx) % NX
        kv_ref[:, y, sx, 2] = sr2[NZ : 2 * NZ, x, y] if dx == 0 else t2[sx, :, y]

    for d in NEAR:
        done(gt.at[(y + NY - d) % NY], rg2.at[d])
    send(gt.at[:, :, oz], gate_ref.at[z], sg3.at[0], rg3.at[0], dev(x, y, oz))
    gate_ref[z] = gt[:, :, z]
    keep0(0)
    keep1(0)
    keep2(0)

    def got20(dy):
        sy = (y + NY - dy) % NY
        for dx in (0, 1, 3, 2):
            done(t0.at[sy, (x + NX - dx) % NX], r20.at[dy, dx])

    def got22(dx):
        for dz in range(NZ):
            done(t2.at[(x + NX - dx) % NX, (z + dz) % NZ], r22.at[dx, dz])

    for dy in NEAR[:2]:
        got20(dy)
        out0(dy)
    got20(2)
    out0(2)
    for dx in NEAR[:2]:
        got22(dx)
        for d in NEAR:
            out2(dx, d)
    for dy in range(NY):
        done(t1.at[oz, (y + NY - dy) % NY], r21.at[dy])
    for d in NEAR:
        out1(1, d)
    got22(2)
    for d in NEAR:
        out2(2, d)
    for d in NEAR:
        keep0(d)
        keep2(d)
    keep1(1)
    done(gate_ref.at[oz], rg3.at[0])

    def local_attend(i, carry):
        attend0(z, i)
        attend2(y, i)
        return carry

    lax.fori_loop(0, NX, local_attend, 0)
    attend1(0, x)
    attend1(1, x)

    def arrive0(dy):
        sy = (y + NY - dy) % NY
        done(kv_ref.at[oz, sy, :, 0], r30.at[dy])
        attend0(oz, sy)

    def arrive1(dz, dx):
        sz, sx = (z + dz) % NZ, (x + NX - dx) % NX
        done(kv_ref.at[sz, :, sx, 1], r31.at[dz, dx])
        attend1(sz, sx)

    def arrive2(dx, dy):
        sx, sy = (x + NX - dx) % NX, (y + NY - dy) % NY
        done(kv_ref.at[:, sy, sx, 2], r32.at[dx, dy])
        attend2(sy, sx)

    arrive0(0)
    for d in NEAR:
        arrive1(0, d)
        arrive2(0, d)
    arrive0(1)
    arrive0(3)
    for dx in NEAR[:2]:
        for d in NEAR:
            arrive2(dx, d)
    arrive0(2)
    for d in NEAR:
        arrive1(1, d)
        arrive2(2, d)

    stat[0:1, :] = m_ref[0:1, :]
    stat[1:2, :] = l_ref[0:1, :]
    stat[2:3, :] = a_ref[0:1, :]
    swap = pltpu.make_async_remote_copy(
        src_ref=stat, dst_ref=peer, send_sem=st.at[0], recv_sem=rt.at[0],
        device_id=(grp, sp, 1 - tp), device_id_type=MESH,
    )
    swap.start()

    for g in range(GROUPS):
        dy, dz = group_step(g)
        yb, zb = py(dy), (z + dz) % NZ
        for d in NEAR:
            done(sr0.at[px(d), yb, zb], s10.at[g, d])
        if dy != 0:
            done(sr1.at[yb, zb], s11.at[g])
        if dz != 0:
            done(sr2.at[zb, :, yb], s12.at[g])
    for d in NEAR:
        for k in range(NX):
            done(t0.at[y, k], s20.at[d, k])
        for k in range(NZ):
            done(t2.at[x, k], s22.at[d, k])
        done(gr.at[x], sg1.at[d])
        done(gt.at[y], sg2.at[d])
        for k in range(NZ):
            done(kv_ref.at[0, :, x, 1], s31.at[k, d])
        for k in range(NX):
            done(kv_ref.at[:, y, 0, 2], s32.at[k, d])
    for k in range(NY):
        done(t1.at[z, k], s21.at[k])
        done(kv_ref.at[z, k, :, 0], s30.at[k])
    done(gate_ref.at[z], sg3.at[0])
    swap.wait()

    mine, theirs = stat[...], peer[...]
    first = jnp.where(tp == 0, mine, theirs)
    second = jnp.where(tp == 0, theirs, mine)
    top = jnp.maximum(first[0:1], second[0:1])
    e1, e2 = jnp.exp(first[0:1] - top), jnp.exp(second[0:1] - top)
    total = first[1:2] * e1 + second[1:2] * e2
    weighted = first[2:3] * e1 + second[2:3] * e2
    read_ref[0] = (weighted / total)[:, half:].astype(BF16)


def store_kernel(kv_ref, gate_ref, read_ref, kv_out, gate_out, read_out, sem):
    copies = []
    for k in range(NZ):
        for j in range(NY):
            copies.append(pltpu.make_async_copy(kv_ref.at[k, j], kv_out.at[k, j], sem.at[len(copies)]))
    copies.append(pltpu.make_async_copy(gate_ref, gate_out, sem.at[len(copies)]))
    copies.append(pltpu.make_async_copy(read_ref, read_out, sem.at[len(copies)]))
    for c in copies:
        c.start()
    for c in copies:
        c.wait()


def on_device(tokens, key_weight, value_weight, cum_gate, query):
    rows, width = tokens.shape[2:]
    hd = query.shape[2]
    unit = rows // COLORS
    cols = NX * hd
    kv_shape = (NZ, NY, NX, COLORS, unit, 2 * hd)
    gate_shape = (NZ, NY, NX, 1, rows)
    read_shape = (1, 1, hd)
    vmem = pl.BlockSpec(memory_space=pltpu.VMEM)
    anywhere = pl.BlockSpec(memory_space=pl.ANY)
    dma = pltpu.SemaphoreType.DMA
    u = (unit, 2 * hd)
    kv, gate, read = pl.pallas_call(
        exchange_kernel,
        out_shape=[pltpu.VMEM(kv_shape, BF16), pltpu.VMEM(gate_shape, F32), pltpu.VMEM(read_shape, BF16)],
        in_specs=[anywhere, anywhere, anywhere, anywhere, vmem],
        out_specs=[vmem, vmem, vmem],
        scratch_shapes=[
            pltpu.VMEM((rows, width), BF16),
            pltpu.VMEM((GROUPS, 2, width, cols), BF16),
            pltpu.VMEM((2 * NX, NY, NZ, *u), BF16),
            pltpu.VMEM((2 * NY, NZ, NX, *u), BF16),
            pltpu.VMEM((2 * NZ, NX, NY, *u), BF16),
            pltpu.VMEM((NY, NX, NZ, *u), BF16),
            pltpu.VMEM((NZ, NY, NX, *u), BF16),
            pltpu.VMEM((NX, NZ, NY, *u), BF16),
            pltpu.VMEM(gate_shape, F32),
            pltpu.VMEM((NX, NZ, NY, 1, rows), F32),
            pltpu.VMEM((NY, NX, NZ, 1, rows), F32),
            pltpu.VMEM((8, 2 * hd), BF16),
            pltpu.VMEM((8, 2 * hd), F32),
            pltpu.VMEM((8, 2 * hd), F32),
            pltpu.VMEM((8, 2 * hd), F32),
            pltpu.VMEM((8, 2 * hd), F32),
            pltpu.VMEM((8, 2 * hd), F32),
            dma(()), dma((GROUPS, 2)), dma((2,)),
            dma((GROUPS, NX)), dma((GROUPS, NX)), dma((GROUPS,)), dma((GROUPS,)), dma((GROUPS,)), dma((GROUPS,)),
            dma((NY, NX)), dma((NY, NX)), dma((NY,)), dma((NY,)), dma((NX, NZ)), dma((NX, NZ)),
            dma((NY,)), dma((NY,)), dma((NZ, NX)), dma((NZ, NX)), dma((NX, NY)), dma((NX, NY)),
            dma((NX,)), dma((NX,)), dma((NY,)), dma((NY,)), dma((1,)), dma((1,)), dma((1,)), dma((1,)),
        ],
        compiler_params=pltpu.CompilerParams(
            collective_id=0, has_side_effects=True, vmem_limit_bytes=50 * 2**20
        ),
        name="exchange",
    )(tokens.reshape(rows, width), key_weight, value_weight, cum_gate.reshape(gate_shape), query.reshape(1, hd))
    kv, gate, read = pl.pallas_call(
        store_kernel,
        out_shape=[
            jax.ShapeDtypeStruct(kv_shape, BF16),
            jax.ShapeDtypeStruct(gate_shape, F32),
            jax.ShapeDtypeStruct(read_shape, BF16),
        ],
        in_specs=[vmem, vmem, vmem],
        out_specs=[anywhere, anywhere, anywhere],
        scratch_shapes=[dma((NZ * NY + 2,))],
        compiler_params=pltpu.CompilerParams(vmem_limit_bytes=2**20),
        name="store",
    )(kv, gate, read)
    length = NX * NY * NZ * rows
    return kv.reshape(1, 1, length, 2 * hd), gate.reshape(1, 1, length), read


def solution(mesh):
    placed = (P("gr", "tp", "sp", None), P(), P(), P("gr", None, "tp", "sp"), P("gr", "sp", None))
    return jax.shard_map(
        on_device,
        mesh=mesh,
        in_specs=placed,
        out_specs=(P("gr", "sp", "tp", None), P("gr", "sp", "tp"), P("gr", "sp", None)),
        check_vma=False,
    )
```

time: 171 us -> 87.7 us (0.51)
  Pallas kernels: 0 us -> 87 us
  blocking collectives: 49.8 us -> 0 us
  local copies, waits for them, and re-layouts: 38.1 us -> 0 us
  waiting for transfers between devices: 32.2 us -> 0 us
  matrix products: 20.9 us -> 0 us
  starting transfers between devices: 14.4 us -> 0 us
  other arithmetic: 9.36 us -> 0 us
  between operations: 4.72 us -> 0.64 us
    pallas_call x0 -> x2, Pallas kernels: none -> 87 us  [the longest x1 84.2 us: on_device(): pl.pallas_call(exchange_kernel, out_shape=[pltpu.VMEM(kv_shape, BF16), pl...]
    all_to_all x1 -> x0, blocking collectives: 44.9 us -> none  [exchange_in_pieces(): lax.all_to_all(share, axis, split_axis=0, concat_axis=0, tiled=True)]
    all_to_all x2 -> x0, waiting for transfers between devices: 32.2 us -> none  [the longest x1 32.2 us: exchange_in_pieces(): lax.all_to_all(share, axis, split_axis=0, concat_axis=0, tiled=True)]
    unnamed x13 -> x0, local copies, waits for them, and re-layouts: 25.3 us -> none
    dot_general x4 -> x0, matrix products: 20.9 us -> none  [the longest x1 9.28 us: local_project(): jnp.einsum('btd,dhe->bhte', local_rows, value_weight.reshape(width, -1, h...]
    all_to_all x2 -> x0, starting transfers between devices: 14.4 us -> none  [the longest x1 9.49 us: on_device(): lax.all_to_all(cum_gate, 'sp', split_axis=1, concat_axis=3, tiled=True)]
    all_to_all x2 -> x0, local copies, waits for them, and re-layouts: 7.49 us -> none  [exchange_in_pieces(): lax.all_to_all(share, axis, split_axis=0, concat_axis=0, tiled=True)]
    all_gather x1 -> x0, blocking collectives: 4.91 us -> none  [gathered_once(): both, at, found = (lax.all_gather(jnp.concatenate(lines), axis), 0, {})]
  transfers between devices with their start and end apart: 2 -> 0, of which waited for: 1 -> 0; matrix products, arithmetic and copies ran while one was open for 31% -> 0% of each run, Pallas kernels for 0% -> 0%
where the time goes in v1:
time: 87.7 us; the launch traced here: 87.6 us
  Pallas kernels  87 us (99%)
    pallas_call x1, Pallas kernels, on_device(): pl.pallas_call(exchange_kernel, out_shape=[pltpu.VMEM(kv_shape, BF16), pl...  84.2 us
    pallas_call x1, Pallas kernels, on_device(): pl.pallas_call(store_kernel, out_shape=[jax.ShapeDtypeStruct(kv_shape, BF...  2.76 us

profile of v1, /device:TPU:1, one launch (start us, length us, event | category | flops | bytes accessed | tf_op | source)
XLA Modules:
  0.0 87.6 jit_solution(6553070918946947528)
XLA Ops:
  0.6 84.2 %exchange.1 = (bf16[2,4,4,3,256,128]{5,4,3,2,1,0:T(8,128)(2,1)S(1)}, f32[2,4,4,1,768]{4,3,2,1,0:T(1,128)S(1)}, bf16[1,1,64]{2,1,0:T(2,128)(2,1)S(1)}) custom-call(bf16[768,2048]{1,0:T(8,128)(2,1)} %bitcast.5, bf16[2048,2048]{1,0:T(8,128)(2,1)} %kw_hbm.1, bf16[2048,2048]{1,0:T(8,128)(2,1)} %vw_hbm.1, f32[2,4,4,1,768]{4,3,2,1,0:T(1,128)} %bitcast.6, ...), custom_call_target="tpu_custom_call" | custom-call | tf_op jit(solution)/shard_map/exchange/pallas_call | solution.py:436
  84.8 2.8 %store.1 = (bf16[2,4,4,3,256,128]{5,4,3,2,1,0:T(8,128)(2,1)}, f32[2,4,4,1,768]{4,3,2,1,0:T(1,128)}, bf16[1,1,64]{2,1,0:T(2,128)(2,1)}) custom-call(bf16[2,4,4,3,256,128]{5,4,3,2,1,0:T(8,128)(2,1)S(1)} %get-tuple-element.9.kv_ref, f32[2,4,4,1,768]{4,3,2,1,0:T(1,128)S(1)} %get-tuple-element.10.gate_ref, bf16[1,1,64]{2,1,0:T(2,128)(2,1)S(1)} %get-tuple-element.11.read_ref), custom_call_target="tpu_custom_call" | custom-call | tf_op jit(solution)/shard_map/store/pallas_call | solution.py:470

commit v2 on v0

v2 whole, which is shorter than its diff:
```python
import functools

import jax
import jax.numpy as jnp
from jax import lax
from jax.experimental import pallas as pl
from jax.experimental.pallas import tpu as pltpu
from jax.sharding import PartitionSpec as P

MESH = pl.DeviceIdType.MESH
NX, NY, NZ = 4, 4, 2
COLORS = 3
GROUPS = NY * NZ
NEAR = (1, 3, 2)
F32 = jnp.float32
BF16 = jnp.bfloat16


def group_step(g):
    h, r = g // 4, g % 4
    dy = (1 - h) * (1 + 2 * (r % 2)) + h * (2 - 2 * (r // 2))
    dz = (1 - h) * (1 - r // 2) + h * (1 - r % 2)
    return dy, dz


def exchange_kernel(
    tok_hbm, kw_hbm, vw_hbm, gate_hbm, q_ref,
    kv_ref, gate_ref, stat, peer,
    tok, w, sr0, sr1, sr2, t0, t1, t2, gin, gr, gt, q8, m_ref, l_ref, a_ref,
    tok_sem, w_sem, gl_sem, out_sem, gs_sem, gd_sem,
    r10, r11, r12, r20, r21, r22, r30, r31, r32, st, rt,
):
    grp, sp, tp = (lax.axis_index(n) for n in ("gr", "sp", "tp"))
    x, y, z = sp % NX, (sp // NX) % NY, sp // (NX * NY)
    oz = 1 - z
    unit = tok.shape[0] // COLORS
    half = q_ref.shape[-1]
    pair = 2 * half
    cols = NX * half
    scale = half ** (-0.5)

    def dev(xx, yy, zz):
        return (grp, zz * (NX * NY) + yy * NX + xx, tp)

    def px(d):
        return (x + d) % NX

    def py(d):
        return (y + d) % NY

    def bx(d):
        return (x + NX - d) % NX

    def by(d):
        return (y + NY - d) % NY

    def send(src, dst, ssem, rsem, to):
        pltpu.make_async_remote_copy(
            src_ref=src, dst_ref=dst, send_sem=ssem, recv_sem=rsem, device_id=to, device_id_type=MESH
        ).start()

    def done(ref, sem):
        pltpu.make_async_copy(ref, ref, sem).wait()

    def load_tokens(c):
        at = pl.ds(c * unit, unit)
        pltpu.make_async_copy(tok_hbm.at[at], tok.at[at], tok_sem.at[c]).start()

    def load_weights(g, h, sem):
        dy, dz = group_step(g)
        at = pl.multiple_of((((z + dz) % NZ) * NY + py(dy)) * cols, cols) + h * pair
        left, right = w.at[g, h, :, pl.ds(0, pair)], w.at[g, h, :, pl.ds(pair, pair)]
        pltpu.make_async_copy(kw_hbm.at[:, pl.ds(at, pair)], left, w_sem.at[sem]).start()
        pltpu.make_async_copy(vw_hbm.at[:, pl.ds(at, pair)], right, w_sem.at[sem]).start()

    def load_group(g):
        load_weights(g, 0, g)
        load_weights(g, 1, g)

    def tokens_here(c):
        done(tok.at[pl.ds(c * unit, unit)], tok_sem.at[c])

    load_weights(0, 0, 0)
    load_tokens(1)
    load_weights(1, 0, 1)
    load_tokens(0)
    load_tokens(2)

    barrier = pltpu.get_barrier_semaphore()
    peers = [dev(px(d), y, z) for d in NEAR] + [dev(x, py(d), z) for d in NEAR]
    peers += [dev(x, y, oz), (grp, sp, 1 - tp)]
    for p in peers:
        pl.semaphore_signal(barrier, inc=1, device_id=p, device_id_type=MESH)

    query = jnp.concatenate([q_ref[...].astype(F32), jnp.zeros((1, half), F32)], axis=-1)
    q8[...] = jnp.broadcast_to(query, q8.shape).astype(BF16)
    m_ref[...] = jnp.full(m_ref.shape, -1e30, F32)
    l_ref[...] = jnp.zeros(l_ref.shape, F32)
    a_ref[...] = jnp.zeros(a_ref.shape, F32)

    lane = lax.broadcasted_iota(jnp.int32, (unit, 2 * half), 1)

    def compute(*steps):
        made = []
        for g, h, c in steps:
            left = tok[c * unit : (c + 1) * unit, :]
            made.append(jnp.dot(left, w[g, h], preferred_element_type=F32))
        for (g, h, c), kv in zip(steps, made):
            dy, dz = group_step(g)
            yb, zb = py(dy), (z + dz) % NZ
            k, v = kv[:, :pair], kv[:, pair:]
            first = jnp.where(lane < half, k, pltpu.roll(v, half, 1)).astype(BF16)
            second = jnp.where(lane < half, pltpu.roll(k, half, 1), v).astype(BF16)
            for j, both in ((2 * h, first), (2 * h + 1, second)):
                if c == 0:
                    sr0[j + NX * (1 - ((j + NX - x) % NX + NX - 1) // NX), yb, zb] = both
                elif c == 1:
                    sr1[yb + NY * (1 - (dy + NY - 1) // NY), zb, j] = both
                else:
                    sr2[zb + NZ * (1 - dz), j, yb] = both

    def half_sends(g, h, c):
        dy, dz = group_step(g)
        yb, zb = py(dy), (z + dz) % NZ
        two = pl.ds(2 * h, 2)
        if c == 0:
            for j in (2 * h, 2 * h + 1):

                @pl.when(x != j)
                def _():
                    d = (j + NX - x) % NX
                    send(sr0.at[j, yb, zb], sr0.at[NX + x, yb, zb], out_sem.at[0], r10.at[dy, d - 1], dev(j, y, z))
        elif c == 1:
            send(sr1.at[yb, zb, two], sr1.at[NY + y, zb, two], out_sem.at[1], r11.at[dy - 1, dz], dev(x, yb, z))
        else:
            send(sr2.at[zb, two, yb], sr2.at[NZ + z, two, yb], out_sem.at[2], r12.at[0], dev(x, y, oz))

    def along_x(dy, dz):
        yb = py(dy)
        at = (yb,) if dz is None else (yb, (z + dz) % NZ)
        for d in NEAR:
            send(
                sr0.at[(px(d), *at)], sr0.at[(NX + x, *at)], out_sem.at[0], r10.at[dy, d - 1], dev(px(d), y, z)
            )

    def along_y(g):
        dy, dz = group_step(g)
        yb, zb = py(dy), (z + dz) % NZ
        send(sr1.at[yb, zb], sr1.at[NY + y, zb], out_sem.at[1], r11.at[dy - 1, dz], dev(x, yb, z))

    def along_z(g):
        yb, zb = py(group_step(g)[0]), oz
        send(sr2.at[zb, :, yb], sr2.at[NZ + z, :, yb], out_sem.at[2], r12.at[0], dev(x, y, oz))

    def whole(g, c):
        compute((g, 0, c), (g, 1, c))

    done(w.at[0, 0], w_sem.at[0])
    tokens_here(1)
    done(w.at[1, 0], w_sem.at[1])
    load_weights(0, 1, GROUPS)
    load_weights(1, 1, GROUPS + 1)
    compute((0, 0, 1), (1, 0, 1))
    pl.semaphore_wait(barrier, len(peers))
    half_sends(0, 0, 1)
    half_sends(1, 0, 1)
    tokens_here(0)
    tokens_here(2)
    load_group(3)
    load_group(2)
    gate_loads = (
        pltpu.make_async_copy(gate_hbm, gin, gl_sem.at[0]),
        pltpu.make_async_copy(gate_hbm.at[:, :, x], gr.at[x], gl_sem.at[1]),
    )
    for load in gate_loads:
        load.start()
    compute((0, 0, 0), (0, 0, 2))
    half_sends(0, 0, 2)
    half_sends(0, 0, 0)
    done(w.at[0, 1], w_sem.at[GROUPS])
    compute((0, 1, 0), (0, 1, 2))
    half_sends(0, 1, 2)
    half_sends(0, 1, 0)
    load_group(4)
    load_group(5)
    done(w.at[1, 1], w_sem.at[GROUPS + 1])
    compute((0, 1, 1), (1, 1, 1))
    half_sends(0, 1, 1)
    half_sends(1, 1, 1)
    for load in gate_loads:
        load.wait()
    for d in NEAR:
        send(gin.at[:, :, px(d)], gr.at[x], gs_sem.at[0], gd_sem.at[0], dev(px(d), y, z))
    whole(1, 0)
    done(w.at[3], w_sem.at[3])
    whole(3, 0)
    along_x(3, None)
    load_group(6)
    load_group(7)
    done(w.at[2], w_sem.at[2])
    whole(2, 1)
    along_y(2)
    whole(3, 1)
    along_y(3)
    whole(1, 2)
    along_z(1)
    whole(2, 0)
    along_x(1, 0)
    done(w.at[4], w_sem.at[4])
    whole(4, 1)
    along_y(4)
    whole(4, 2)
    along_z(4)
    whole(4, 0)
    done(w.at[5], w_sem.at[5])
    whole(5, 0)
    along_x(2, None)
    done(gr.at[0 : NX - 1], gd_sem.at[0])
    gt[y] = gr[:, :, y]
    for d in NEAR:
        send(gr.at[:, :, py(d)], gt.at[y], gs_sem.at[1], gd_sem.at[1], dev(x, py(d), z))
    whole(5, 1)
    along_y(5)
    done(w.at[6], w_sem.at[6])
    whole(6, 2)
    along_z(6)
    whole(6, 0)
    done(w.at[7], w_sem.at[7])
    whole(7, 0)
    along_x(0, None)
    for g, c in ((6, 1), (7, 1), (2, 2), (3, 2), (5, 2), (7, 2)):
        whole(g, c)

    def fwd0(dy, dx):
        send(sr0.at[NX + bx(dx), py(dy)], t0.at[y, bx(dx)], out_sem.at[0], r20.at[dy - 1], dev(x, py(dy), z))

    def fwd1(dy):
        send(sr1.at[NY + by(dy), oz], t1.at[z, by(dy)], out_sem.at[1], r21.at[0], dev(x, y, oz))

    def fwd2(dx, dz):
        sz = (z + dz) % NZ
        send(sr2.at[NZ + sz, px(dx)], t2.at[x, sz], out_sem.at[2], r22.at[dx - 1], dev(px(dx), y, z))

    def got10(dy, dx):
        done(sr0.at[NX + bx(dx), py(dy)], r10.at[dy, dx - 1])

    def got11(dy, dz):
        done(sr1.at[NY + by(dy), (z + dz) % NZ], r11.at[dy - 1, dz])

    def got20(dy):
        done(t0.at[by(dy)], r20.at[dy - 1])

    def got22(dx):
        done(t2.at[bx(dx)], r22.at[dx - 1])

    def out0(dy):
        src = sr0.at[pl.ds(NX, NX), y, oz] if dy == 0 else t0.at[by(dy), :, oz]
        send(src, kv_ref.at[z, by(dy), :, 0], out_sem.at[0], r30.at[dy], dev(x, y, oz))

    def out1(dz, dx):
        sz = (z + dz) % NZ
        src = sr1.at[pl.ds(NY, NY), z, px(dx)] if dz == 0 else t1.at[sz, :, px(dx)]
        send(src, kv_ref.at[sz, :, x, 1], out_sem.at[1], r31.at[dz, dx - 1], dev(px(dx), y, z))

    def out2(dx, dy):
        src = sr2.at[pl.ds(NZ, NZ), x, py(dy)] if dx == 0 else t2.at[bx(dx), :, py(dy)]
        send(src, kv_ref.at[:, y, bx(dx), 2], out_sem.at[2], r32.at[dx, dy - 1], dev(x, py(dy), z))

    def keep0(dy):
        kv_ref[z, by(dy), :, 0] = sr0[NX : 2 * NX, y, z] if dy == 0 else t0[by(dy), :, z]

    def keep1(dz):
        sz = (z + dz) % NZ
        kv_ref[sz, :, x, 1] = sr1[NY : 2 * NY, z, x] if dz == 0 else t1[sz, :, x]

    def keep2(dx):
        kv_ref[:, y, bx(dx), 2] = sr2[NZ : 2 * NZ, x, y] if dx == 0 else t2[bx(dx), :, y]

    def come0(dy):
        done(kv_ref.at[oz, by(dy), :, 0], r30.at[dy])

    def come1(dz, dx):
        done(kv_ref.at[(z + dz) % NZ, :, bx(dx), 1], r31.at[dz, dx - 1])

    def come2(dx, dy):
        done(kv_ref.at[:, by(dy), bx(dx), 2], r32.at[dx, dy - 1])

    def part0(sz, sy):
        gates = [gate_ref[sz, sy, k, :, 0:unit] for k in range(NX)]
        return kv_ref[sz, sy, :, 0].reshape(NX * unit, 2 * half), gates

    def part1(sz, sx):
        gates = [gate_ref[sz, k, sx, :, unit : 2 * unit] for k in range(NY)]
        return kv_ref[sz, :, sx, 1].reshape(NY * unit, 2 * half), gates

    def part2(sy, sx):
        gates = [gate_ref[k, sy, sx, :, 2 * unit : 3 * unit] for k in range(NZ)]
        return kv_ref[:, sy, sx, 2].reshape(NZ * unit, 2 * half), gates

    def folded(op, values):
        width = 2 * half
        pieces = [v[:, i : i + width] for v in values for i in range(0, v.shape[1], width)]
        while len(pieces) > 1:
            pieces = [op(*pieces[i : i + 2]) if i + 1 < len(pieces) else pieces[i] for i in range(0, len(pieces), 2)]
        return pieces[0]

    def attend(parts):
        scores = []
        for kv, gates in parts:
            s = lax.dot_general(q8[...], kv, (((1,), (1,)), ((), ())), preferred_element_type=F32)
            scores.append(s * scale - jnp.concatenate(gates, axis=-1))
        old = m_ref[...]
        top = jnp.maximum(old, jnp.max(folded(jnp.maximum, scores), axis=1, keepdims=True))
        weights = [jnp.exp(s - top[:, :1]) for s in scores]
        keep = jnp.exp(old - top)
        m_ref[...] = top
        l_ref[...] = l_ref[...] * keep + jnp.sum(folded(jnp.add, weights), axis=1, keepdims=True)
        acc = a_ref[...] * keep
        for p, (kv, _) in zip(weights, parts):
            acc = acc + jnp.dot(p.astype(BF16), kv, preferred_element_type=F32)
        a_ref[...] = acc

    fwd1(0)
    for d in NEAR:
        if d != 2:
            fwd0(d, 0)
        fwd2(d, 0)
    done(gt.at[0 : NY - 1], gd_sem.at[1])
    send(gt.at[:, :, oz], gate_ref.at[z], gs_sem.at[2], gd_sem.at[2], dev(x, y, oz))
    gate_ref[z] = gt[:, :, z]
    for dy in NEAR[:2]:
        got11(dy, 1)
        fwd1(dy)
    for dx in NEAR:
        for dy in NEAR[:2]:
            got10(dy, dx)
            fwd0(dy, dx)
    got11(2, 1)
    fwd1(2)
    for dx in NEAR:
        got10(2, dx)
    send(sr0.at[pl.ds(NX, NX), py(2)], t0.at[y], out_sem.at[0], r20.at[1], dev(x, py(2), z))
    done(sr2.at[NZ + oz], r12.at[0])
    for dx in NEAR:
        fwd2(dx, 1)
    for dx in NEAR:
        got10(0, dx)
    out0(0)
    for dy in NEAR:
        got11(dy, 0)
    for d in NEAR:
        out1(0, d)
        out2(0, d)
    keep0(0)
    keep1(0)
    keep2(0)
    done(gate_ref.at[oz], gd_sem.at[2])
    attend([part0(z, y), part1(z, x), part2(y, x)])

    for dy in NEAR[:2]:
        got20(dy)
        out0(dy)
    for dy in NEAR[:2]:
        keep0(dy)
    attend([part0(z, by(1)), part0(z, by(3))])
    for dx in NEAR[:2]:
        got22(dx)
        for d in NEAR:
            out2(dx, d)
    got20(2)
    out0(2)
    done(t1.at[oz], r21.at[0])
    for d in NEAR:
        out1(1, d)
    got22(2)
    for d in NEAR:
        out2(2, d)
    keep0(2)
    keep1(1)
    for d in NEAR:
        keep2(d)
    attend([part0(z, by(2)), part1(oz, x)] + [part2(y, bx(d)) for d in NEAR])

    come0(0)
    come1(0, 1)
    come1(0, 3)
    for d in NEAR:
        come2(0, d)
    attend([part0(oz, y), part1(z, bx(1)), part1(z, bx(3))] + [part2(by(d), x) for d in NEAR])
    come0(1)
    come1(0, 2)
    for d in NEAR:
        come2(1, d)
    attend([part0(oz, by(1)), part1(z, bx(2))] + [part2(by(d), bx(1)) for d in NEAR])
    come0(3)
    come1(1, 1)
    come1(1, 3)
    for d in NEAR:
        come2(3, d)
    attend([part0(oz, by(3)), part1(oz, bx(1)), part1(oz, bx(3))] + [part2(by(d), bx(3)) for d in NEAR])
    come2(2, 1)
    come2(2, 3)
    attend([part2(by(1), bx(2)), part2(by(3), bx(2))])
    come0(2)
    come1(1, 2)
    come2(2, 2)
    attend([part0(oz, by(2)), part1(oz, bx(2)), part2(by(2), bx(2))])

    stat[0:1, :] = m_ref[0:1, :]
    stat[1:2, :] = l_ref[0:1, :]
    stat[2:3, :] = a_ref[0:1, :]
    swap = pltpu.make_async_remote_copy(
        src_ref=stat, dst_ref=peer, send_sem=st.at[0], recv_sem=rt.at[0],
        device_id=(grp, sp, 1 - tp), device_id_type=MESH,
    )
    swap.start()
    done(sr0, out_sem.at[0])
    done(sr1, out_sem.at[1])
    done(sr2, out_sem.at[2])
    done(gr.at[0 : NX - 1], gs_sem.at[0])
    done(gt.at[0 : NY - 1], gs_sem.at[1])
    done(gate_ref.at[z], gs_sem.at[2])
    swap.wait()


def store_kernel(kv_ref, gate_ref, stat, peer, kv_out, gate_out, read_out, read_ref, sem):
    copies = [
        pltpu.make_async_copy(kv_ref.at[k, j], kv_out.at[k, j], sem.at[0]) for k in range(NZ) for j in range(NY)
    ]
    copies.append(pltpu.make_async_copy(gate_ref, gate_out, sem.at[1]))
    for c in copies:
        c.start()
    half = read_ref.shape[-1]
    tp = lax.axis_index("tp")
    first = jnp.where(tp == 0, stat[...], peer[...])
    second = jnp.where(tp == 0, peer[...], stat[...])
    top = jnp.maximum(first[0:1], second[0:1])
    e1, e2 = jnp.exp(first[0:1] - top), jnp.exp(second[0:1] - top)
    total = first[1:2] * e1 + second[1:2] * e2
    weighted = first[2:3] * e1 + second[2:3] * e2
    read_ref[0] = (weighted / total)[:, half:].astype(BF16)
    last = pltpu.make_async_copy(read_ref, read_out, sem.at[2])
    last.start()
    pltpu.make_async_copy(kv_ref, kv_out, sem.at[0]).wait()
    copies[-1].wait()
    last.wait()


def on_device(tokens, key_weight, value_weight, cum_gate, query):
    rows, width = tokens.shape[2:]
    hd = query.shape[2]
    unit = rows // COLORS
    cols = NX * hd
    kv_shape = (NZ, NY, NX, COLORS, unit, 2 * hd)
    gate_shape = (NZ, NY, NX, 1, rows)
    read_shape = (1, 1, hd)
    vmem = pl.BlockSpec(memory_space=pltpu.VMEM)
    anywhere = pl.BlockSpec(memory_space=pl.ANY)
    dma = pltpu.SemaphoreType.DMA
    u = (unit, 2 * hd)
    stat_shape = (8, 2 * hd)
    kv, gate, stat, peer = pl.pallas_call(
        exchange_kernel,
        out_shape=[
            pltpu.VMEM(kv_shape, BF16),
            pltpu.VMEM(gate_shape, F32),
            pltpu.VMEM(stat_shape, F32),
            pltpu.VMEM(stat_shape, F32),
        ],
        in_specs=[anywhere, anywhere, anywhere, anywhere, vmem],
        out_specs=[vmem, vmem, vmem, vmem],
        scratch_shapes=[
            pltpu.VMEM((rows, width), BF16),
            pltpu.VMEM((GROUPS, 2, width, cols), BF16),
            pltpu.VMEM((2 * NX, NY, NZ, *u), BF16),
            pltpu.VMEM((2 * NY, NZ, NX, *u), BF16),
            pltpu.VMEM((2 * NZ, NX, NY, *u), BF16),
            pltpu.VMEM((NY, NX, NZ, *u), BF16),
            pltpu.VMEM((NZ, NY, NX, *u), BF16),
            pltpu.VMEM((NX, NZ, NY, *u), BF16),
            pltpu.VMEM(gate_shape, F32),
            pltpu.VMEM((NX, NZ, NY, 1, rows), F32),
            pltpu.VMEM((NY, NX, NZ, 1, rows), F32),
            pltpu.VMEM((8, 2 * hd), BF16),
            pltpu.VMEM(stat_shape, F32),
            pltpu.VMEM(stat_shape, F32),
            pltpu.VMEM(stat_shape, F32),
            dma((COLORS,)), dma((GROUPS + 2,)), dma((2,)), dma((COLORS,)), dma((3,)), dma((3,)),
            dma((NY, NX - 1)), dma((NY - 1, NZ)), dma((1,)),
            dma((NY - 1,)), dma((1,)), dma((NX - 1,)),
            dma((NY,)), dma((NZ, NX - 1)), dma((NX, NY - 1)), dma((1,)), dma((1,)),
        ],
        compiler_params=pltpu.CompilerParams(
            collective_id=0, has_side_effects=True, vmem_limit_bytes=50 * 2**20
        ),
        name="exchange",
    )(tokens.reshape(rows, width), key_weight, value_weight, cum_gate.reshape(gate_shape), query.reshape(1, hd))
    kv, gate, read = pl.pallas_call(
        store_kernel,
        out_shape=[
            jax.ShapeDtypeStruct(kv_shape, BF16),
            jax.ShapeDtypeStruct(gate_shape, F32),
            jax.ShapeDtypeStruct(read_shape, BF16),
        ],
        in_specs=[vmem] * 4,
        out_specs=[anywhere, anywhere, anywhere],
        scratch_shapes=[pltpu.VMEM(read_shape, BF16), dma((3,))],
        compiler_params=pltpu.CompilerParams(vmem_limit_bytes=2**20),
        name="store",
    )(kv, gate, stat, peer)
    length = NX * NY * NZ * rows
    return kv.reshape(1, 1, length, 2 * hd), gate.reshape(1, 1, length), read


def solution(mesh):
    placed = (P("gr", "tp", "sp", None), P(), P(), P("gr", None, "tp", "sp"), P("gr", "sp", None))
    return jax.shard_map(
        on_device,
        mesh=mesh,
        in_specs=placed,
        out_specs=(P("gr", "sp", "tp", None), P("gr", "sp", "tp"), P("gr", "sp", None)),
        check_vma=False,
    )
```

time: 171 us -> 84.1 us (0.49)
  Pallas kernels: 0 us -> 83.1 us
  blocking collectives: 49.8 us -> 0 us
  local copies, waits for them, and re-layouts: 38.1 us -> 0 us
  waiting for transfers between devices: 32.2 us -> 0 us
  matrix products: 20.9 us -> 0 us
  starting transfers between devices: 14.4 us -> 0 us
  other arithmetic: 9.36 us -> 0 us
  between operations: 4.72 us -> 0.8 us
    pallas_call x0 -> x2, Pallas kernels: none -> 83.1 us  [the longest x1 80.4 us: on_device(): pl.pallas_call(exchange_kernel, out_shape=[pltpu.VMEM(kv_shape, BF16), pl...]
    all_to_all x1 -> x0, blocking collectives: 44.9 us -> none  [exchange_in_pieces(): lax.all_to_all(share, axis, split_axis=0, concat_axis=0, tiled=True)]
    all_to_all x2 -> x0, waiting for transfers between devices: 32.2 us -> none  [the longest x1 32.2 us: exchange_in_pieces(): lax.all_to_all(share, axis, split_axis=0, concat_axis=0, tiled=True)]
    unnamed x13 -> x0, local copies, waits for them, and re-layouts: 25.3 us -> none
    dot_general x4 -> x0, matrix products: 20.9 us -> none  [the longest x1 9.28 us: local_project(): jnp.einsum('btd,dhe->bhte', local_rows, value_weight.reshape(width, -1, h...]
    all_to_all x2 -> x0, starting transfers between devices: 14.4 us -> none  [the longest x1 9.49 us: on_device(): lax.all_to_all(cum_gate, 'sp', split_axis=1, concat_axis=3, tiled=True)]
    all_to_all x2 -> x0, local copies, waits for them, and re-layouts: 7.49 us -> none  [exchange_in_pieces(): lax.all_to_all(share, axis, split_axis=0, concat_axis=0, tiled=True)]
    all_gather x1 -> x0, blocking collectives: 4.91 us -> none  [gathered_once(): both, at, found = (lax.all_gather(jnp.concatenate(lines), axis), 0, {})]
  transfers between devices with their start and end apart: 2 -> 0, of which waited for: 1 -> 0; matrix products, arithmetic and copies ran while one was open for 31% -> 0% of each run, Pallas kernels for 0% -> 0%
where the time goes in v2:
time: 84.1 us; the launch traced here: 83.9 us
  Pallas kernels  83.1 us (99%)
    pallas_call x1, Pallas kernels, on_device(): pl.pallas_call(exchange_kernel, out_shape=[pltpu.VMEM(kv_shape, BF16), pl...  80.4 us
    pallas_call x1, Pallas kernels, on_device(): pl.pallas_call(store_kernel, out_shape=[jax.ShapeDtypeStruct(kv_shape, BF...  2.7 us

profile of v2, /device:TPU:1, one launch (start us, length us, event | category | flops | bytes accessed | tf_op | source)
XLA Modules:
  0.0 83.9 jit_solution(12354951395973272603)
XLA Ops:
  0.6 80.4 %exchange.1 = (bf16[2,4,4,3,256,128]{5,4,3,2,1,0:T(8,128)(2,1)S(1)}, f32[2,4,4,1,768]{4,3,2,1,0:T(1,128)S(1)}, f32[8,128]{1,0:T(8,128)S(1)}, f32[8,128]{1,0:T(8,128)S(1)}) custom-call(bf16[768,2048]{1,0:T(8,128)(2,1)} %bitcast.5, bf16[2048,2048]{1,0:T(8,128)(2,1)} %kw_hbm.1, bf16[2048,2048]{1,0:T(8,128)(2,1)} %vw_hbm.1, f32[2,4,4,1,768]{4,3,2,1,0:T(1,128)} %bitcast.6, ...), custom_call_target="tpu_custom_call" | custom-call | tf_op jit(solution)/shard_map/exchange/pallas_call | solution.py:462
  81.1 2.7 %store.1 = (bf16[2,4,4,3,256,128]{5,4,3,2,1,0:T(8,128)(2,1)}, f32[2,4,4,1,768]{4,3,2,1,0:T(1,128)}, bf16[1,1,64]{2,1,0:T(2,128)(2,1)}) custom-call(bf16[2,4,4,3,256,128]{5,4,3,2,1,0:T(8,128)(2,1)S(1)} %get-tuple-element.10.kv_ref, f32[2,4,4,1,768]{4,3,2,1,0:T(1,128)S(1)} %get-tuple-element.11.gate_ref, f32[8,128]{1,0:T(8,128)S(1)} %get-tuple-element.12.stat, ...), custom_call_target="tpu_custom_call" | custom-call | tf_op jit(solution)/shard_map/store/pallas_call | solution.py:498

commit v3 on v2

--- a/solution.py
+++ b/solution.py
@@ -12,6 +12,10 @@
 COLORS = 3
 GROUPS = NY * NZ
 NEAR = (1, 3, 2)
+WAY_X1 = (3, 1, 1, 3)
+WAY_Y1 = (3, 1)
+WAY_X = (1, 3)
+WAY_Y = (1, 1, 3, 3)
 F32 = jnp.float32
 BF16 = jnp.bfloat16
 
@@ -26,8 +30,10 @@
 def exchange_kernel(
     tok_hbm, kw_hbm, vw_hbm, gate_hbm, q_ref,
     kv_ref, gate_ref, stat, peer,
-    tok, w, sr0, sr1, sr2, t0, t1, t2, gin, gr, gt, q8, m_ref, l_ref, a_ref,
-    tok_sem, w_sem, gl_sem, out_sem, gs_sem, gd_sem,
+    tok, w, sr0, sr1, sr2, t0, t1, t2, qx1, qy1, qx2, qy2, qx3, qy3,
+    gin, gr, gt, q8, m_ref, l_ref, a_ref,
+    tok_sem, w_sem, gl_sem, out_sem, hop_sem, gs_sem, gd_sem,
+    hx1, hy1, hx2, hy2, hx3, hy3,
     r10, r11, r12, r20, r21, r22, r30, r31, r32, st, rt,
 ):
     grp, sp, tp = (lax.axis_index(n) for n in ("gr", "sp", "tp"))
@@ -84,6 +90,7 @@
     load_tokens(1)
     load_weights(1, 0, 1)
     load_tokens(0)
+    load_weights(0, 1, GROUPS)
     load_tokens(2)
 
     barrier = pltpu.get_barrier_semaphore()
@@ -119,127 +126,158 @@
                 else:
                     sr2[zb + NZ * (1 - dz), j, yb] = both
 
-    def half_sends(g, h, c):
+    def whole(g, c):
+        compute((g, 0, c), (g, 1, c))
+
+    def block(dy, dz):
+        return (py(dy),) if dz is None else (py(dy), (z + dz) % NZ)
+
+    def stop_x1(dy, dz):
+        return (dy,) if dz is None else (dy, (z + dz) % NZ)
+
+    def along_x(dy, dz):
+        at = block(dy, dz)
+        for d in (1, 3):
+            send(sr0.at[(px(d), *at)], sr0.at[(NX + x, *at)], out_sem.at[0], r10.at[dy, d - 1], dev(px(d), y, z))
+        s = WAY_X1[dy]
+        stop = qx1.at[stop_x1(dy, dz)]
+        send(sr0.at[(px(2), *at)], stop, out_sem.at[0], hx1.at[dy, dz or 0], dev(px(s), y, z))
+
+    def relay_x1(dy, dz):
+        s = WAY_X1[dy]
+        stop = qx1.at[stop_x1(dy, dz)]
+        done(stop, hx1.at[dy, dz or 0])
+        send(stop, sr0.at[(NX + bx(s), *block(dy, dz))], hop_sem.at[0], r10.at[dy, 1], dev(px(s), y, z))
+
+    def along_y(g, two=slice(None)):
         dy, dz = group_step(g)
         yb, zb = py(dy), (z + dz) % NZ
-        two = pl.ds(2 * h, 2)
-        if c == 0:
-            for j in (2 * h, 2 * h + 1):
-
-                @pl.when(x != j)
-                def _():
-                    d = (j + NX - x) % NX
-                    send(sr0.at[j, yb, zb], sr0.at[NX + x, yb, zb], out_sem.at[0], r10.at[dy, d - 1], dev(j, y, z))
-        elif c == 1:
-            send(sr1.at[yb, zb, two], sr1.at[NY + y, zb, two], out_sem.at[1], r11.at[dy - 1, dz], dev(x, yb, z))
-        else:
-            send(sr2.at[zb, two, yb], sr2.at[NZ + z, two, yb], out_sem.at[2], r12.at[0], dev(x, y, oz))
-
-    def along_x(dy, dz):
-        yb = py(dy)
-        at = (yb,) if dz is None else (yb, (z + dz) % NZ)
-        for d in NEAR:
-            send(
-                sr0.at[(px(d), *at)], sr0.at[(NX + x, *at)], out_sem.at[0], r10.at[dy, d - 1], dev(px(d), y, z)
-            )
-
-    def along_y(g):
-        dy, dz = group_step(g)
-        yb, zb = py(dy), (z + dz) % NZ
-        send(sr1.at[yb, zb], sr1.at[NY + y, zb], out_sem.at[1], r11.at[dy - 1, dz], dev(x, yb, z))
+        send(sr1.at[yb, zb, two], sr1.at[NY + y, zb, two], out_sem.at[1], r11.at[dy - 1, dz], dev(x, yb, z))
+
+    def start_y1(dz):
+        to = dev(x, py(WAY_Y1[dz]), z)
+        send(sr1.at[py(2), (z + dz) % NZ], qy1.at[dz], out_sem.at[1], hy1.at[dz], to)
+
+    def relay_y1(dz):
+        s = WAY_Y1[dz]
+        done(qy1.at[dz], hy1.at[dz])
+        send(qy1.at[dz], sr1.at[NY + by(s), (z + dz) % NZ], hop_sem.at[0], r11.at[1, dz], dev(x, py(s), z))
 
     def along_z(g):
-        yb, zb = py(group_step(g)[0]), oz
-        send(sr2.at[zb, :, yb], sr2.at[NZ + z, :, yb], out_sem.at[2], r12.at[0], dev(x, y, oz))
-
-    def whole(g, c):
-        compute((g, 0, c), (g, 1, c))
+        yb = py(group_step(g)[0])
+        send(sr2.at[oz, :, yb], sr2.at[NZ + z, :, yb], out_sem.at[2], r12.at[0], dev(x, y, oz))
 
     done(w.at[0, 0], w_sem.at[0])
     tokens_here(1)
     done(w.at[1, 0], w_sem.at[1])
-    load_weights(0, 1, GROUPS)
     load_weights(1, 1, GROUPS + 1)
     compute((0, 0, 1), (1, 0, 1))
     pl.semaphore_wait(barrier, len(peers))
-    half_sends(0, 0, 1)
-    half_sends(1, 0, 1)
+    along_y(0, pl.ds(0, 2))
+    along_y(1, pl.ds(0, 2))
     tokens_here(0)
-    tokens_here(2)
+    done(w.at[0, 1], w_sem.at[GROUPS])
     load_group(3)
-    load_group(2)
+    load_group(4)
     gate_loads = (
         pltpu.make_async_copy(gate_hbm, gin, gl_sem.at[0]),
         pltpu.make_async_copy(gate_hbm.at[:, :, x], gr.at[x], gl_sem.at[1]),
     )
     for load in gate_loads:
         load.start()
-    compute((0, 0, 0), (0, 0, 2))
-    half_sends(0, 0, 2)
-    half_sends(0, 0, 0)
-    done(w.at[0, 1], w_sem.at[GROUPS])
-    compute((0, 1, 0), (0, 1, 2))
-    half_sends(0, 1, 2)
-    half_sends(0, 1, 0)
-    load_group(4)
+    whole(0, 0)
+    along_x(1, 1)
+    tokens_here(2)
+    whole(0, 2)
+    along_z(0)
+    done(w.at[1, 1], w_sem.at[GROUPS + 1])
+    whole(1, 0)
+    along_x(3, 1)
+    compute((0, 1, 1), (1, 1, 1))
+    along_y(0, pl.ds(2, 2))
+    along_y(1, pl.ds(2, 2))
     load_group(5)
-    done(w.at[1, 1], w_sem.at[GROUPS + 1])
-    compute((0, 1, 1), (1, 1, 1))
-    half_sends(0, 1, 1)
-    half_sends(1, 1, 1)
+    load_group(2)
     for load in gate_loads:
         load.wait()
     for d in NEAR:
         send(gin.at[:, :, px(d)], gr.at[x], gs_sem.at[0], gd_sem.at[0], dev(px(d), y, z))
-    whole(1, 0)
     done(w.at[3], w_sem.at[3])
     whole(3, 0)
-    along_x(3, None)
+    along_x(3, 0)
+    done(w.at[4], w_sem.at[4])
+    whole(4, 1)
+    start_y1(1)
+    done(w.at[5], w_sem.at[5])
+    whole(5, 1)
+    start_y1(0)
     load_group(6)
     load_group(7)
+    whole(1, 2)
+    along_z(1)
     done(w.at[2], w_sem.at[2])
+    whole(2, 0)
+    along_x(1, 0)
     whole(2, 1)
     along_y(2)
     whole(3, 1)
     along_y(3)
-    whole(1, 2)
-    along_z(1)
-    whole(2, 0)
-    along_x(1, 0)
-    done(w.at[4], w_sem.at[4])
-    whole(4, 1)
-    along_y(4)
-    whole(4, 2)
-    along_z(4)
+    relay_x1(1, 1)
+    relay_x1(3, 1)
     whole(4, 0)
-    done(w.at[5], w_sem.at[5])
     whole(5, 0)
     along_x(2, None)
     done(gr.at[0 : NX - 1], gd_sem.at[0])
     gt[y] = gr[:, :, y]
     for d in NEAR:
         send(gr.at[:, :, py(d)], gt.at[y], gs_sem.at[1], gd_sem.at[1], dev(x, py(d), z))
-    whole(5, 1)
-    along_y(5)
+    whole(4, 2)
+    along_z(4)
     done(w.at[6], w_sem.at[6])
-    whole(6, 2)
-    along_z(6)
     whole(6, 0)
     done(w.at[7], w_sem.at[7])
     whole(7, 0)
     along_x(0, None)
-    for g, c in ((6, 1), (7, 1), (2, 2), (3, 2), (5, 2), (7, 2)):
-        whole(g, c)
+    relay_x1(3, 0)
+    relay_x1(1, 0)
+    whole(6, 2)
+    along_z(6)
+    whole(6, 1)
+    whole(7, 1)
+    whole(2, 2)
+    relay_y1(1)
+    relay_y1(0)
+    whole(3, 2)
+    whole(5, 2)
+    whole(7, 2)
 
     def fwd0(dy, dx):
-        send(sr0.at[NX + bx(dx), py(dy)], t0.at[y, bx(dx)], out_sem.at[0], r20.at[dy - 1], dev(x, py(dy), z))
+        src = sr0.at[NX + bx(dx), py(dy)]
+        if dy == 2:
+            send(src, qy2.at[dx], out_sem.at[0], hy2.at[dx], dev(x, py(WAY_Y[dx]), z))
+        else:
+            send(src, t0.at[y, bx(dx)], out_sem.at[0], r20.at[dy - 1], dev(x, py(dy), z))
+
+    def relay_y2(dx):
+        s = WAY_Y[dx]
+        done(qy2.at[dx], hy2.at[dx])
+        send(qy2.at[dx], t0.at[by(s), bx(dx)], hop_sem.at[1], r20.at[1], dev(x, py(s), z))
 
     def fwd1(dy):
         send(sr1.at[NY + by(dy), oz], t1.at[z, by(dy)], out_sem.at[1], r21.at[0], dev(x, y, oz))
 
     def fwd2(dx, dz):
         sz = (z + dz) % NZ
-        send(sr2.at[NZ + sz, px(dx)], t2.at[x, sz], out_sem.at[2], r22.at[dx - 1], dev(px(dx), y, z))
+        src = sr2.at[NZ + sz, px(dx)]
+        if dx == 2:
+            send(src, qx2.at[dz], out_sem.at[2], hx2.at[dz], dev(px(WAY_X[dz]), y, z))
+        else:
+            send(src, t2.at[x, sz], out_sem.at[2], r22.at[dx - 1], dev(px(dx), y, z))
+
+    def relay_x2(dz):
+        s = WAY_X[dz]
+        done(qx2.at[dz], hx2.at[dz])
+        send(qx2.at[dz], t2.at[bx(s), (z + dz) % NZ], hop_sem.at[1], r22.at[1], dev(px(s), y, z))
 
     def got10(dy, dx):
         done(sr0.at[NX + bx(dx), py(dy)], r10.at[dy, dx - 1])
@@ -260,11 +298,27 @@
     def out1(dz, dx):
         sz = (z + dz) % NZ
         src = sr1.at[pl.ds(NY, NY), z, px(dx)] if dz == 0 else t1.at[sz, :, px(dx)]
-        send(src, kv_ref.at[sz, :, x, 1], out_sem.at[1], r31.at[dz, dx - 1], dev(px(dx), y, z))
+        if dx == 2:
+            send(src, qx3.at[dz], out_sem.at[1], hx3.at[dz], dev(px(WAY_X[dz]), y, z))
+        else:
+            send(src, kv_ref.at[sz, :, x, 1], out_sem.at[1], r31.at[dz, dx - 1], dev(px(dx), y, z))
+
+    def relay_x3(dz):
+        s = WAY_X[dz]
+        done(qx3.at[dz], hx3.at[dz])
+        send(qx3.at[dz], kv_ref.at[(z + dz) % NZ, :, bx(s), 1], hop_sem.at[2], r31.at[dz, 1], dev(px(s), y, z))
 
     def out2(dx, dy):
         src = sr2.at[pl.ds(NZ, NZ), x, py(dy)] if dx == 0 else t2.at[bx(dx), :, py(dy)]
-        send(src, kv_ref.at[:, y, bx(dx), 2], out_sem.at[2], r32.at[dx, dy - 1], dev(x, py(dy), z))
+        if dy == 2:
+            send(src, qy3.at[dx], out_sem.at[2], hy3.at[dx], dev(x, py(WAY_Y[dx]), z))
+        else:
+            send(src, kv_ref.at[:, y, bx(dx), 2], out_sem.at[2], r32.at[dx, dy - 1], dev(x, py(dy), z))
+
+    def relay_y3(dx):
+        s = WAY_Y[dx]
+        done(qy3.at[dx], hy3.at[dx])
+        send(qy3.at[dx], kv_ref.at[:, by(s), bx(dx), 2], hop_sem.at[2], r32.at[dx, 1], dev(x, py(s), z))
 
     def keep0(dy):
         kv_ref[z, by(dy), :, 0] = sr0[NX : 2 * NX, y, z] if dy == 0 else t0[by(dy), :, z]
@@ -321,90 +375,108 @@
         a_ref[...] = acc
 
     fwd1(0)
-    for d in NEAR:
-        if d != 2:
-            fwd0(d, 0)
-        fwd2(d, 0)
+    fwd0(1, 0)
+    fwd0(3, 0)
+    fwd0(2, 0)
+    for dy in (1, 3):
+        got11(dy, 1)
+        fwd1(dy)
+    relay_x1(2, None)
+    fwd2(2, 0)
+    fwd2(1, 0)
+    fwd2(3, 0)
+    for dx in (1, 3):
+        for dy in (1, 3, 2):
+            got10(dy, dx)
+            fwd0(dy, dx)
+    for dy in (1, 3):
+        got10(dy, 2)
+        fwd0(dy, 2)
+    relay_x1(0, None)
     done(gt.at[0 : NY - 1], gd_sem.at[1])
     send(gt.at[:, :, oz], gate_ref.at[z], gs_sem.at[2], gd_sem.at[2], dev(x, y, oz))
     gate_ref[z] = gt[:, :, z]
-    for dy in NEAR[:2]:
-        got11(dy, 1)
-        fwd1(dy)
-    for dx in NEAR:
-        for dy in NEAR[:2]:
-            got10(dy, dx)
-            fwd0(dy, dx)
     got11(2, 1)
     fwd1(2)
-    for dx in NEAR:
-        got10(2, dx)
-    send(sr0.at[pl.ds(NX, NX), py(2)], t0.at[y], out_sem.at[0], r20.at[1], dev(x, py(2), z))
     done(sr2.at[NZ + oz], r12.at[0])
-    for dx in NEAR:
+    for dx in (2, 1, 3):
         fwd2(dx, 1)
     for dx in NEAR:
         got10(0, dx)
     out0(0)
     for dy in NEAR:
         got11(dy, 0)
-    for d in NEAR:
-        out1(0, d)
-        out2(0, d)
     keep0(0)
     keep1(0)
     keep2(0)
-    done(gate_ref.at[oz], gd_sem.at[2])
-    attend([part0(z, y), part1(z, x), part2(y, x)])
-
-    for dy in NEAR[:2]:
+    attend([part0(z, y), part1(z, x)])
+    relay_x2(0)
+    got10(2, 2)
+    fwd0(2, 2)
+    relay_y2(0)
+    relay_y2(3)
+    relay_y2(1)
+    relay_x2(1)
+    relay_y2(2)
+    for d in (2, 1, 3):
+        out1(0, d)
+        out2(0, d)
+    for dy in (1, 3):
         got20(dy)
         out0(dy)
-    for dy in NEAR[:2]:
-        keep0(dy)
+    keep0(1)
+    keep0(3)
     attend([part0(z, by(1)), part0(z, by(3))])
-    for dx in NEAR[:2]:
+    for dx in (1, 3):
         got22(dx)
-        for d in NEAR:
+        for d in (2, dx, 4 - dx):
             out2(dx, d)
     got20(2)
     out0(2)
     done(t1.at[oz], r21.at[0])
-    for d in NEAR:
+    for d in (2, 3, 1):
         out1(1, d)
     got22(2)
-    for d in NEAR:
+    for d in (2, 3, 1):
         out2(2, d)
+    relay_y3(0)
     keep0(2)
     keep1(1)
     for d in NEAR:
         keep2(d)
-    attend([part0(z, by(2)), part1(oz, x)] + [part2(y, bx(d)) for d in NEAR])
+    done(gate_ref.at[oz], gd_sem.at[2])
+    attend([part0(z, by(2)), part1(oz, x)] + [part2(y, bx(d)) for d in range(NX)])
+    relay_x3(0)
 
     come0(0)
+    come1(0, 3)
+    for dx, dy in ((0, 3), (0, 1), (1, 3)):
+        come2(dx, dy)
+    attend([part0(oz, y), part1(z, bx(3)), part2(by(3), x), part2(by(1), x), part2(by(3), bx(1))])
+    relay_y3(3)
+    relay_y3(1)
+    relay_x3(1)
+    come0(1)
     come1(0, 1)
-    come1(0, 3)
-    for d in NEAR:
-        come2(0, d)
-    attend([part0(oz, y), part1(z, bx(1)), part1(z, bx(3))] + [part2(by(d), x) for d in NEAR])
-    come0(1)
-    come1(0, 2)
-    for d in NEAR:
-        come2(1, d)
-    attend([part0(oz, by(1)), part1(z, bx(2))] + [part2(by(d), bx(1)) for d in NEAR])
+    for dx, dy in ((1, 1), (3, 3), (3, 1)):
+        come2(dx, dy)
+    attend([part0(oz, by(1)), part1(z, bx(1)), part2(by(1), bx(1)), part2(by(3), bx(3)), part2(by(1), bx(3))])
+    relay_y3(2)
     come0(3)
-    come1(1, 1)
     come1(1, 3)
-    for d in NEAR:
-        come2(3, d)
-    attend([part0(oz, by(3)), part1(oz, bx(1)), part1(oz, bx(3))] + [part2(by(d), bx(3)) for d in NEAR])
     come2(2, 1)
     come2(2, 3)
-    attend([part2(by(1), bx(2)), part2(by(3), bx(2))])
+    attend([part0(oz, by(3)), part1(oz, bx(3)), part2(by(1), bx(2)), part2(by(3), bx(2))])
+    come1(1, 1)
+    come2(0, 2)
+    come2(3, 2)
+    come2(1, 2)
+    come2(2, 2)
+    attend([part1(oz, bx(1))] + [part2(by(2), bx(d)) for d in range(NX)])
     come0(2)
+    come1(0, 2)
     come1(1, 2)
-    come2(2, 2)
-    attend([part0(oz, by(2)), part1(oz, bx(2)), part2(by(2), bx(2))])
+    attend([part0(oz, by(2)), part1(z, bx(2)), part1(oz, bx(2))])
 
     stat[0:1, :] = m_ref[0:1, :]
     stat[1:2, :] = l_ref[0:1, :]
@@ -417,6 +489,8 @@
     done(sr0, out_sem.at[0])
     done(sr1, out_sem.at[1])
     done(sr2, out_sem.at[2])
+    for k in range(3):
+        done(t0.at[0:2], hop_sem.at[k])
     done(gr.at[0 : NX - 1], gs_sem.at[0])
     done(gt.at[0 : NY - 1], gs_sem.at[1])
     done(gate_ref.at[z], gs_sem.at[2])
@@ -478,6 +552,12 @@
             pltpu.VMEM((NY, NX, NZ, *u), BF16),
             pltpu.VMEM((NZ, NY, NX, *u), BF16),
             pltpu.VMEM((NX, NZ, NY, *u), BF16),
+            pltpu.VMEM((NY, NZ, *u), BF16),
+            pltpu.VMEM((NZ, NX, *u), BF16),
+            pltpu.VMEM((NZ, NY, *u), BF16),
+            pltpu.VMEM((NX, NZ, *u), BF16),
+            pltpu.VMEM((NZ, NY, *u), BF16),
+            pltpu.VMEM((NX, NZ, *u), BF16),
             pltpu.VMEM(gate_shape, F32),
             pltpu.VMEM((NX, NZ, NY, 1, rows), F32),
             pltpu.VMEM((NY, NX, NZ, 1, rows), F32),
@@ -485,7 +565,8 @@
             pltpu.VMEM(stat_shape, F32),
             pltpu.VMEM(stat_shape, F32),
             pltpu.VMEM(stat_shape, F32),
-            dma((COLORS,)), dma((GROUPS + 2,)), dma((2,)), dma((COLORS,)), dma((3,)), dma((3,)),
+            dma((COLORS,)), dma((GROUPS + 2,)), dma((2,)), dma((COLORS,)), dma((3,)), dma((3,)), dma((3,)),
+            dma((NY, NZ)), dma((NZ,)), dma((NZ,)), dma((NX,)), dma((NZ,)), dma((NX,)),
             dma((NY, NX - 1)), dma((NY - 1, NZ)), dma((1,)),
             dma((NY - 1,)), dma((1,)), dma((NX - 1,)),
             dma((NY,)), dma((NZ, NX - 1)), dma((NX, NY - 1)), dma((1,)), dma((1,)),

time: 84.1 us -> 84 us (level)
  no operation moved by 1% of the time
where the time goes in v3:
time: 84 us; the launch traced here: 83.8 us
  Pallas kernels  83 us (99%)
    pallas_call x1, Pallas kernels, on_device(): pl.pallas_call(exchange_kernel, out_shape=[pltpu.VMEM(kv_shape, BF16), pl...  80.3 us
    pallas_call x1, Pallas kernels, on_device(): pl.pallas_call(store_kernel, out_shape=[jax.ShapeDtypeStruct(kv_shape, BF...  2.7 us

profile of v3, /device:TPU:1, one launch (start us, length us, event | category | flops | bytes accessed | tf_op | source)
XLA Modules:
  0.0 83.8 jit_solution(14435567082323599350)
XLA Ops:
  0.6 80.3 %exchange.1 = (bf16[2,4,4,3,256,128]{5,4,3,2,1,0:T(8,128)(2,1)S(1)}, f32[2,4,4,1,768]{4,3,2,1,0:T(1,128)S(1)}, f32[8,128]{1,0:T(8,128)S(1)}, f32[8,128]{1,0:T(8,128)S(1)}) custom-call(bf16[768,2048]{1,0:T(8,128)(2,1)} %bitcast.5, bf16[2048,2048]{1,0:T(8,128)(2,1)} %kw_hbm.1, bf16[2048,2048]{1,0:T(8,128)(2,1)} %vw_hbm.1, f32[2,4,4,1,768]{4,3,2,1,0:T(1,128)} %bitcast.6, ...), custom_call_target="tpu_custom_call" | custom-call | tf_op jit(solution)/shard_map/exchange/pallas_call | solution.py:536
  81.0 2.7 %store.1 = (bf16[2,4,4,3,256,128]{5,4,3,2,1,0:T(8,128)(2,1)}, f32[2,4,4,1,768]{4,3,2,1,0:T(1,128)}, bf16[1,1,64]{2,1,0:T(2,128)(2,1)}) custom-call(bf16[2,4,4,3,256,128]{5,4,3,2,1,0:T(8,128)(2,1)S(1)} %get-tuple-element.10.kv_ref, f32[2,4,4,1,768]{4,3,2,1,0:T(1,128)S(1)} %get-tuple-element.11.gate_ref, f32[8,128]{1,0:T(8,128)S(1)} %get-tuple-element.12.stat, ...), custom_call_target="tpu_custom_call" | custom-call | tf_op jit(solution)/shard_map/store/pallas_call | solution.py:579
